TPU v7x, 32 devices: a whole 2x2x4 slice. The times are simulated.
32 devices in a mesh: ep: 8 (over z, core), tp: 4 (over y, x).
Axes of the slice: x: 2, y: 2, z: 4, core: 2. Of those that a mesh axis runs over, the one named last changes fastest.
Arguments:
- queries: bfloat16 [4096, 1024], P('ep', 'tp'), may hold values from -9 to 9
- keys: bfloat16 [4096, 128], P('ep'), may hold values from -6 to 6
- values: bfloat16 [4096, 128], P('ep'), may hold values from -6 to 6
- sink_logits: float32 [16], P('tp'), may hold values from 2 to 7
- out_weight: bfloat16 [1024, 2048], P(None, 'tp'), may hold values from -0.8984375 to 0.8984375
- expert_input: bfloat16 [2048, 2048], P('ep'), may hold values from -6 to 6
- norm_gain: float32 [2048], replicated, may hold values from 0.1 to 1.9
- routes: int32 [2048, 2], P('ep'), may hold values from 0 to 7, all different within a row; in each aligned block of 256 rows (0 to 255, 256 to 511, ...) at most 128 rows name the same one
- route_weights: float32 [2048, 2], P('ep'), may hold values from 0.1 to 1
- gate_weight: bfloat16 [8, 2048, 4096], P('ep', None, 'tp'), may hold values from -0.125 to 0.125
- up_weight: bfloat16 [8, 2048, 4096], P('ep', None, 'tp'), may hold values from -0.125 to 0.125
- down_weight: bfloat16 [8, 4096, 2048], P('ep', 'tp'), may hold values from -0.09375 to 0.09375
Outputs:
- attn_out: bfloat16 [4096, 2048], P('ep', 'tp')
- expert_out: bfloat16 [2048, 2048], P('ep', 'tp')
Inputs may be any that keep to these rules, and one draw needn't show every extreme that they name: `routes`: each row names 2 different experts. Within the rows of one index of ep (aligned blocks of 256 rows) no expert is named by more than 128 rows, and in some blocks one expert is named by exactly 128 rows.
All inputs are finite; a program needn't handle non-finite values.
Results may differ from a plain program's by a relative error of at most 0.015.
Values may be sent and summed in bfloat16 or wider, within the bound.
A program may use at most 64 MiB of HBM per device.

v0:
```python
import jax
import jax.numpy as jnp
from jax import lax
from jax.sharding import PartitionSpec as P

HEADS = 16
KV = 2
HD = 64
WINDOW = 128
rms_eps = 1e-06
mask_value = -1e30


def passed_along(value, axis, steps):
    count = lax.axis_size(axis)
    first, last = (max(0, -steps), min(count, count - steps))
    return lax.ppermute(value, axis, [(source, source + steps) for source in range(first, last)])


def rotate_heads(values_in, positions):
    half_dim = values_in.shape[-1] // 2
    inv_freq = 10000.0 ** (-jnp.arange(half_dim, dtype=jnp.float32) * (2.0 / values_in.shape[-1]))
    angles = positions[:, None] * inv_freq[None, :]
    cosine_table = jnp.cos(angles)[:, None, :]
    sine_table = jnp.sin(angles)[:, None, :]
    first_half = values_in[..., :half_dim]
    second_half = values_in[..., half_dim:]
    return jnp.concatenate(
        [
            first_half * cosine_table - second_half * sine_table,
            second_half * cosine_table + first_half * sine_table,
        ],
        axis=-1,
    )


def local(
    queries,
    keys,
    values,
    sink_logits,
    out_weight,
    expert_input,
    norm_gain,
    routes,
    route_weights,
    gate_weight,
    up_weight,
    down_weight,
):
    seq_rows = queries.shape[0]
    heads_here = queries.shape[1] // HD
    group_size = HEADS // KV
    kv_here = max(1, heads_here // group_size)
    heads_per_kv = heads_here // kv_here
    kv_first = lax.axis_index("tp") * heads_here // group_size
    key_local = lax.dynamic_slice_in_dim(keys, kv_first * HD, kv_here * HD, 1)
    value_local = lax.dynamic_slice_in_dim(values, kv_first * HD, kv_here * HD, 1)
    offset = lax.axis_index("ep") * seq_rows
    positions = (offset + jnp.arange(seq_rows, dtype=jnp.int32)).astype(jnp.float32)
    query_rot = rotate_heads(
        queries.astype(jnp.float32).reshape(seq_rows, heads_here, HD), positions
    ).astype(jnp.bfloat16)
    key_rot = rotate_heads(
        key_local.astype(jnp.float32).reshape(seq_rows, kv_here, HD), positions
    ).astype(jnp.bfloat16)
    value_heads = value_local.reshape(seq_rows, kv_here, HD)
    rim_pair = jnp.concatenate(
        [
            key_rot.reshape(seq_rows, kv_here * HD)[seq_rows - WINDOW :],
            value_local[seq_rows - WINDOW :],
        ],
        axis=1,
    )
    rim_pair = passed_along(rim_pair, "ep", 1)
    rim_key = rim_pair[:, : kv_here * HD].reshape(WINDOW, kv_here, HD)
    rim_value = rim_pair[:, kv_here * HD :].reshape(WINDOW, kv_here, HD)
    blocks = seq_rows // WINDOW

    def band_of(rim_part, local_part):
        padded = jnp.concatenate([rim_part, local_part], axis=0)
        earlier = padded[:seq_rows].reshape(blocks, WINDOW, kv_here, HD)
        current = padded[WINDOW:].reshape(blocks, WINDOW, kv_here, HD)
        return jnp.concatenate([earlier, current], axis=1)

    key_band = band_of(rim_key, key_rot)
    value_band = band_of(rim_value, value_heads)
    query_blocks = query_rot.reshape(blocks, WINDOW, kv_here, heads_per_kv, HD)
    scores = jnp.einsum(
        "nqhgd,nkhd->nhgqk", query_blocks, key_band, preferred_element_type=jnp.float32
    ) * HD ** (-0.5)
    block_start = offset + jnp.arange(blocks, dtype=jnp.int32)[:, None, None] * WINDOW
    query_pos = block_start + jnp.arange(WINDOW, dtype=jnp.int32)[None, :, None]
    key_pos = block_start - WINDOW + jnp.arange(2 * WINDOW, dtype=jnp.int32)[None, None, :]
    distance = query_pos - key_pos
    allowed = (distance >= 0) & (distance < WINDOW) & (key_pos >= 0)
    scores = jnp.where(allowed[:, None, None], scores, mask_value)
    sink_row = sink_logits.reshape(1, kv_here, heads_per_kv, 1)
    row_top = jnp.maximum(jnp.max(scores, axis=-1), sink_row)
    exp_scores = jnp.exp(scores - row_top[..., None])
    row_total = jnp.sum(exp_scores, axis=-1) + jnp.exp(sink_row - row_top)
    weights = (exp_scores / row_total[..., None]).astype(jnp.bfloat16)
    head_mix = jnp.einsum(
        "nhgqk,nkhd->nqhgd", weights, value_band, preferred_element_type=jnp.float32
    )
    head_mix = head_mix.astype(jnp.bfloat16).reshape(seq_rows, heads_here * HD)
    attn_out = jnp.dot(
        lax.all_gather(head_mix, "tp", axis=1, tiled=True),
        out_weight,
        preferred_element_type=jnp.float32,
    ).astype(jnp.bfloat16)
    token_rows = expert_input.shape[0]
    top_count = routes.shape[1]
    expert_count = lax.axis_size("ep")
    capacity = 2 * top_count * token_rows // expert_count
    slot_total = expert_count * capacity
    input_wide = expert_input.astype(jnp.float32)
    inv_rms = lax.rsqrt(jnp.mean(input_wide * input_wide, axis=-1, keepdims=True) + rms_eps)
    normed = (input_wide * inv_rms * norm_gain[None, :]).astype(jnp.bfloat16)
    flat_expert = routes.reshape(-1)
    one_hot = (flat_expert[:, None] == jnp.arange(expert_count, dtype=jnp.int32)[None, :]).astype(
        jnp.int32
    )
    route_rank = jnp.sum(jnp.cumsum(one_hot, axis=0) * one_hot, axis=1) - 1
    slot_of_route = flat_expert * capacity + route_rank
    matches = slot_of_route[None, :] == jnp.arange(slot_total, dtype=jnp.int32)[:, None]
    route_token = jnp.arange(token_rows * top_count, dtype=jnp.int32) // top_count
    source_row = jnp.sum(jnp.where(matches, route_token[None, :] + 1, 0), axis=1) - 1
    occupied = source_row >= 0
    gate_local = gate_weight[0]
    up_local = up_weight[0]
    down_local = down_weight[0]
    column_count = normed.shape[1] // lax.axis_size("tp")
    own_columns = lax.dynamic_slice_in_dim(
        normed, lax.axis_index("tp") * column_count, column_count, 1
    )
    slot_rows = jnp.where(
        occupied[:, None],
        jnp.take(own_columns, jnp.maximum(source_row, 0), axis=0),
        jnp.zeros((), jnp.bfloat16),
    )
    outgoing = slot_rows.reshape(expert_count, capacity, column_count)
    arrived = lax.all_to_all(outgoing, "ep", split_axis=0, concat_axis=0, tiled=True)
    leading = arrived.shape[:2]
    portion = lax.all_gather(arrived, "tp", axis=2, tiled=True)
    flat_piece = portion.reshape(-1, portion.shape[2])
    gate_acc = jnp.dot(flat_piece, gate_local, preferred_element_type=jnp.float32)
    up_acc = jnp.dot(flat_piece, up_local, preferred_element_type=jnp.float32)
    hidden = (jax.nn.silu(gate_acc) * up_acc).astype(jnp.bfloat16)
    summed = lax.psum_scatter(
        lax.dot_general(
            down_local, hidden, (((0,), (1,)), ((), ())), preferred_element_type=jnp.float32
        ).astype(jnp.bfloat16),
        "tp",
        scatter_dimension=0,
        tiled=True,
    ).astype(jnp.float32)
    returned = summed.astype(jnp.bfloat16).reshape((summed.shape[0],) + leading)
    results_home = lax.all_to_all(returned, "ep", split_axis=1, concat_axis=1, tiled=True)
    home_flat = results_home.reshape(results_home.shape[0], -1)
    picked = jnp.take(home_flat, slot_of_route, axis=1).astype(jnp.float32)
    weighted = picked * route_weights.reshape(1, -1)
    combined = jnp.sum(weighted.reshape(results_home.shape[0], token_rows, top_count), axis=2)
    expert_out = combined.T.astype(jnp.bfloat16)
    return (attn_out, expert_out)


def solution(mesh):
    return jax.shard_map(
        local,
        mesh=mesh,
        in_specs=(
            P("ep", "tp"),
            P("ep", None),
            P("ep", None),
            P("tp"),
            P(None, "tp"),
            P("ep", None),
            P(),
            P("ep", None),
            P("ep", None),
            P("ep", None, "tp"),
            P("ep", None, "tp"),
            P("ep", "tp", None),
        ),
        out_specs=(P("ep", "tp"), P("ep", "tp")),
        check_vma=False,
    )
```

profile of v0, /device:TPU:0, one launch (start us, length us, event | category | flops | bytes accessed | tf_op | source)
XLA Modules:
  0.0 217.6 jit_solution(8200057702894979410)
XLA Ops:
  7.2 0.0 copy-start
  7.2 0.0 all-gather.5.cloned.1.call-start
  7.2 1.5 convert_element_type.82
  8.8 1.5 multiply_reduce_fusion
  10.3 0.1 copy.80
  10.4 0.1 eq.39
  10.6 0.1 reshape.508
  10.7 1.1 reduce-window.6
  11.9 0.2 slice_reduce_fusion
  12.1 0.1 fusion.39
  12.2 0.3 select_reduce_fusion
  12.6 0.8 dynamic-slice
  13.4 0.1 fusion.14
  13.5 4.0 %gather_fusion = bf16[1024,512]{1,0:T(8,128)(2,1)S(1)} fusion(bf16[256,512]{1,0:T(8,128)(2,1)S(1)} %fusion.14, s32[1024]{0:T(1024)S(1)} %maximum_clamp_fusion), kind=kCustom, calls=%fused_computation | custom fusion | bytes 2101248 | tf_op jit(solution)/shard_map/jit(_take)/gather | solution.py:139
  17.5 0.5 select_select_fusion
  17.9 32.8 %all_to_all.10 = bf16[8,128,512]{2,1,0:T(8,128)(2,1)} all-to-all(bf16[8,128,512]{2,1,0:T(8,128)(2,1)S(1)} %select_select_fusion), channel_id=1, replica_groups=mesh['ep'=8,'tp'=4] {'ep'}, dimensions={0} | all-to-all | bytes 2097152 | tf_op jit(solution)/shard_map/all_to_all | solution.py:143
  50.7 0.0 all-gather.5.cloned.1.call-update
  50.8 0.0 reduce-scatter.2.cloned.1.call-start
  50.8 51.5 %all-gather.5.cloned.1.call-done = bf16[8,128,2048]{2,1,0:T(8,128)(2,1)} async-done(((bf16[8,128,512]{2,1,0:T(8,128)(2,1)}), bf16[8,128,2048]{2,1,0:T(8,128)(2,1)}) %all-gather.5.cloned.1.call-update) | async-done | bytes 4194320 | tf_op jit(solution)/shard_map/all_gather | solution.py:145
  102.3 7.6 %fusion.2 = f32[1024,1024]{1,0:T(8,128)S(1)} fusion(bf16[1024,2048]{1,0:T(8,128)(2,1)} %bitcast.127, bf16[1,2048,1024]{2,1,0:T(8,128)(2,1)} %param.22), kind=kOutput, calls=%fused_computation.4 | convolution fusion | flops 4294967296 | bytes 12582912 | tf_op jit(solution)/shard_map/dot_general | solution.py:148
  110.0 0.0 copy-start.8
  110.0 5.4 %multiply_convert_fusion = bf16[1024,1024]{1,0:T(8,128)(2,1)S(1)} fusion(f32[1024,1024]{1,0:T(8,128)S(1)} %fusion.2, bf16[1024,2048]{1,0:T(8,128)(2,1)S(1)} %bitcast.128, bf16[1,2048,1024]{2,1,0:T(8,128)(2,1)S(1)} %copy-done.7), kind=kOutput, calls=%fused_computation.9 | convolution fusion | flops 4301258752 | bytes 14680064 | tf_op jit(solution)/shard_map/dot_general | solution.py:147
  115.4 6.1 %convert_bitcast_fusion = bf16[2048,1024]{0,1:T(8,128)(2,1)} fusion(bf16[1024,1024]{1,0:T(8,128)(2,1)S(1)} %multiply_convert_fusion, bf16[1,1024,2048]{2,1,0:T(8,128)(2,1)S(1)} %copy-done.8), kind=kOutput, calls=%fused_computation.8 | convolution fusion | flops 4297064448 | bytes 10485760 | tf_op jit(solution)/shard_map/dot_general | solution.py:151
  121.4 0.0 reduce-scatter.2.cloned.1.call-update
  121.5 0.0 copy-start.6
  121.5 0.0 all-gather.3.cloned.1.call-start
  121.5 0.8 copy-done.2
  122.3 0.1 copy-done.3
  122.4 0.1 constant_dynamic-slice_fusion
  122.5 0.1 copy.89
  122.7 0.1 copy.90
  122.8 0.3 fusion.33
  123.2 1.6 collective-permute-start
  124.8 0.1 copy.75
  124.9 0.1 convert.25
  125.0 0.1 broadcast_compare_fusion
  125.1 0.1 iota_add_fusion.1
  125.1 0.1 iota_add_fusion
  125.2 0.3 multiply_cosine_fusion
  125.5 0.3 fusion.16
  125.9 0.1 fusion.20
  126.1 0.0 collective-permute-done
  126.1 0.5 fusion.47
  126.6 0.1 broadcast_maximum_fusion
  126.7 0.3 fusion.10
  127.0 0.1 exponential_add_fusion
  127.1 0.5 fusion.11
  127.6 0.2 copy.79
  127.8 0.7 copy.105
  128.6 0.0 all-gather.3.cloned.1.call-update
  128.6 45.6 %reduce-scatter.2.cloned.1.call-done = bf16[512,1024]{0,1:T(8,128)(2,1)} async-done(((bf16[2048,1024]{0,1:T(8,128)(2,1)}), bf16[512,1024]{0,1:T(8,128)(2,1)}) %reduce-scatter.2.cloned.1.call-update) | async-done | bytes 1048592 | tf_op jit(solution)/shard_map/reduce_scatter | solution.py:150
  174.2 4.6 %all-to-all-start.1 = ((bf16[512,8,128]{0,2,1:T(8,128)(2,1)}), bf16[512,8,128]{0,2,1:T(8,128)(2,1)S(1)}, u32[]{:S(2)}, u32[]{:S(2)}) async-start(bf16[512,8,128]{0,2,1:T(8,128)(2,1)} %bitcast.120), calls=%async_computation.2 | async-start | bytes 2097152 | tf_op jit(solution)/shard_map/all_to_all | solution.py:159
  178.8 0.1 copy.84
  179.0 0.1 mul.228
  179.1 0.1 sub.79
  179.3 0.1 copy.82
  179.4 0.2 copy.83
  179.6 0.1 copy.85
  179.7 23.4 %all-gather.3.cloned.1.call-done = bf16[512,1024]{0,1:T(8,128)(2,1)} async-done(((bf16[512,256]{0,1:T(8,128)(2,1)}), bf16[512,1024]{0,1:T(8,128)(2,1)}) %all-gather.3.cloned.1.call-update) | async-done | bytes 1048592 | tf_op jit(solution)/shard_map/all_gather | solution.py:108
  203.2 2.8 %convolution_convert_fusion = bf16[512,512]{1,0:T(8,128)(2,1)} fusion(bf16[512,1024]{0,1:T(8,128)(2,1)} %all-gather.3.cloned.1.call-done, bf16[1024,512]{1,0:T(8,128)(2,1)S(1)} %copy-done), kind=kOutput, calls=%fused_computation.17 | convolution fusion | flops 537133056 | bytes 2621440 | tf_op jit(solution)/shard_map/dot_general | solution.py:107
  205.9 0.0 all-to-all-done.1
  205.9 2.0 gather_fusion.1
  207.9 0.2 gather.15
  208.1 2.9 %multiply_reduce_fusion.1 = bf16[512,256]{0,1:T(8,128)(2,1)} fusion(bf16[512,256,2]{0,2,1:T(2,128)(2,1)S(1)} %gather.15, pred[256,2]{1,0:T(8,128)(4,1)S(1)} %copy.83, f32[256,2]{1,0:T(8,128)S(1)} %copy.85), kind=kLoop, calls=%fused_computation.21 | loop fusion | flops 917504 | bytes 788992 | tf_op jit(solution)/shard_map/reduce_sum | solution.py:163
  (41 shorter events, 0.3 us)
Async XLA Ops:
  7.2 196.0 %copy-start = (bf16[1024,512]{1,0:T(8,128)(2,1)S(1)}, bf16[1024,512]{1,0:T(8,128)(2,1)}, u32[]{:S(2)}) copy-start(bf16[1024,512]{1,0:T(8,128)(2,1)} %param.16) | copy-start | bytes 3145732
  7.2 3.1 %copy-start.4 = (s32[256,2]{0,1:T(2,128)S(1)}, s32[256,2]{0,1:T(2,128)}, u32[]{:S(2)}) copy-start(s32[256,2]{0,1:T(2,128)} %param.19) | copy-start | bytes 6148
  7.2 95.1 %all-gather.5.cloned.1.call-start = ((), (), s32[]{:S(2)}) async-start(), calls=%async_computation.4 | async-start | bytes 5242880 | tf_op jit(solution)/shard_map/all_gather | solution.py:145
  50.8 123.5 %reduce-scatter.2.cloned.1.call-start = ((), (), s32[]{:S(2)}) async-start(), calls=%async_computation.5 | async-start | bytes 5242880 | tf_op jit(solution)/shard_map/reduce_scatter | solution.py:150
  102.3 7.7 %copy-start.7 = (bf16[1,2048,1024]{2,1,0:T(8,128)(2,1)S(1)}, bf16[1,2048,1024]{2,1,0:T(8,128)(2,1)}, u32[]{:S(2)}) copy-start(bf16[1,2048,1024]{2,1,0:T(8,128)(2,1)} %param.21) | copy-start | bytes 12582916
  102.3 7.7 %copy-start.9 = (bf16[8,128,2048]{2,1,0:T(8,128)(2,1)S(1)}, bf16[8,128,2048]{2,1,0:T(8,128)(2,1)}, u32[]{:S(2)}) copy-start(bf16[8,128,2048]{2,1,0:T(8,128)(2,1)} %all-gather.5.cloned.1.call-done) | copy-start | bytes 12582916
  110.0 5.4 %copy-start.8 = (bf16[1,1024,2048]{2,1,0:T(8,128)(2,1)S(1)}, bf16[1,1024,2048]{2,1,0:T(8,128)(2,1)}, u32[]{:S(2)}) copy-start(bf16[1,1024,2048]{2,1,0:T(8,128)(2,1)} %param.23) | copy-start | bytes 12582916
  121.4 0.9 copy-start.2
  121.4 1.0 copy-start.3
  121.4 3.3 %copy-start.1 = (bf16[512,256]{1,0:T(8,128)(2,1)S(1)}, bf16[512,256]{1,0:T(8,128)(2,1)}, u32[]{:S(2)}) copy-start(bf16[512,256]{1,0:T(8,128)(2,1)} %param.12) | copy-start | bytes 786436
  121.5 5.2 %copy-start.6 = (f32[4]{0:T(128)S(1)}, f32[4]{0:T(128)}, u32[]{:S(2)}) copy-start(f32[4]{0:T(128)} %param.15) | copy-start | bytes 52
  121.5 81.7 %all-gather.3.cloned.1.call-start = ((), (), s32[]{:S(2)}) async-start(), calls=%async_computation.3 | async-start | bytes 1310720 | tf_op jit(solution)/shard_map/all_gather | solution.py:108
  123.2 2.9 %collective-permute-start = (bf16[128,128]{0,1:T(8,128)(2,1)S(1)}, bf16[128,128]{0,1:T(8,128)(2,1)S(1)}, u32[]{:S(2)}, u32[]{:S(2)}) collective-permute-start(bf16[128,128]{0,1:T(8,128)(2,1)S(1)} %pad_maximum_fusion.3), channel_id=1, source_target_pairs={{0,4},{4,8},{8,12},{12,16},{16,20},{20,24},{24,28},{1,5},{5,9},{9,... | collective-permute-start | bytes 98312 | tf_op jit(solution)/shard_map/ppermute | solution.py:17
  127.1 52.5 %copy-start.5 = (f32[256,2]{0,1:T(2,128)S(1)}, f32[256,2]{0,1:T(2,128)}, u32[]{:S(2)}) copy-start(f32[256,2]{0,1:T(2,128)} %param.20) | copy-start | bytes 6148
  174.2 31.7 %all-to-all-start.1 = ((bf16[512,8,128]{0,2,1:T(8,128)(2,1)}), bf16[512,8,128]{0,2,1:T(8,128)(2,1)S(1)}, u32[]{:S(2)}, u32[]{:S(2)}) async-start(bf16[512,8,128]{0,2,1:T(8,128)(2,1)} %bitcast.120), calls=%async_computation.2 | async-start | bytes 2097152 | tf_op jit(solution)/shard_map/all_to_all | solution.py:159
Sparse Core Ops, SparseCore 0:
  50.9 51.3 all-gather.4
  121.6 52.5 reduce-scatter.1
  176.6 26.4 all-gather.2
where the time goes:
time: 218 us
  waiting for transfers between devices  121 us (56%)
  blocking collectives  32.8 us (15%)
  matrix products  22.8 us (10%)
  between operations  14.2 us (7%)
  local copies, waits for them, and re-layouts  10.8 us (5%)
  other arithmetic  10 us (5%)
  starting transfers between devices  6.3 us (3%)
    all_gather x1, waiting for transfers between devices, local(): portion = lax.all_gather(arrived, 'tp', axis=2, tiled=True)  51.5 us
    reduce_scatter x1, waiting for transfers between devices, local(): lax.psum_scatter(lax.dot_general(down_local, hidden, (((0,), (1,)), ((),...  45.6 us
    all_to_all x1, blocking collectives, local(): lax.all_to_all(outgoing, 'ep', split_axis=0, concat_axis=0, tiled=True)  32.8 us
    all_gather x1, waiting for transfers between devices, local(): lax.all_gather(head_mix, 'tp', axis=1, tiled=True)  23.4 us
    dot_general x1, matrix products, local(): up_acc = jnp.dot(flat_piece, up_local, preferred_element_type=jnp.float32)  7.64 us
    dot_general x1, matrix products, local(): lax.dot_general(down_local, hidden, (((0,), (1,)), ((), ())), preferred_e...  6.07 us
    dot_general x1, matrix products, local(): jnp.dot(flat_piece, gate_local, preferred_element_type=jnp.float32)  5.35 us
    all_to_all x1, starting transfers between devices, local(): lax.all_to_all(returned, 'ep', split_axis=1, concat_axis=1, tiled=True)  4.61 us
  transfers between devices with their start and end apart: 5, of which 3 were waited for; matrix products, arithmetic and copies ran while one was open for 4% of the time, Pallas kernels for 0%

commit v1 on v0

--- a/solution.py
+++ b/solution.py
@@ -142,7 +142,9 @@
     outgoing = slot_rows.reshape(expert_count, capacity, column_count)
     arrived = lax.all_to_all(outgoing, "ep", split_axis=0, concat_axis=0, tiled=True)
     leading = arrived.shape[:2]
-    portion = lax.all_gather(arrived, "tp", axis=2, tiled=True)
+    portion = jnp.concatenate(
+        lax.all_to_all(jnp.stack([arrived] * lax.axis_size("tp")), "tp", 0, 0), axis=2
+    )
     flat_piece = portion.reshape(-1, portion.shape[2])
     gate_acc = jnp.dot(flat_piece, gate_local, preferred_element_type=jnp.float32)
     up_acc = jnp.dot(flat_piece, up_local, preferred_element_type=jnp.float32)

time: 218 us -> 225 us (1.032)
  waiting for transfers between devices: 121 us -> 67.3 us
  blocking collectives: 32.8 us -> 84 us
  matrix products: 22.8 us -> 26.1 us
  local copies, waits for them, and re-layouts: 10.8 us -> 14 us
  other arithmetic: 10 us -> 12.4 us
    all_gather x1 -> x0, waiting for transfers between devices: 51.5 us -> none  [local(): portion = lax.all_gather(arrived, 'tp', axis=2, tiled=True)]
    all_to_all x0 -> x1, blocking collectives: none -> 51.3 us  [local(): lax.all_to_all(jnp.stack([arrived] * lax.axis_size('tp')), 'tp', 0, 0)]
    dot_general x1, matrix products: 6.07 us -> 16.3 us  [local(): lax.dot_general(down_local, hidden, (((0,), (1,)), ((), ())), preferred_e...]
    dot_general x1 -> x0, matrix products: 5.35 us -> none  [local(): jnp.dot(flat_piece, gate_local, preferred_element_type=jnp.float32)]
  transfers between devices with their start and end apart: 5 -> 4, of which waited for: 3 -> 2; matrix products, arithmetic and copies ran while one was open for 4% -> 4% of each run, Pallas kernels for 0% -> 0%
where the time goes in v1:
time: 225 us; the launch traced here: 224 us
  blocking collectives  84 us (37%)
  waiting for transfers between devices  67.3 us (30%)
  matrix products  26.1 us (12%)
  between operations  14.5 us (6%)
  local copies, waits for them, and re-layouts  14 us (6%)
  other arithmetic  12.4 us (6%)
  starting transfers between devices  6.16 us (3%)
    all_to_all x1, blocking collectives, local(): lax.all_to_all(jnp.stack([arrived] * lax.axis_size('tp')), 'tp', 0, 0)  51.3 us
    reduce_scatter x1, waiting for transfers between devices, local(): lax.psum_scatter(lax.dot_general(down_local, hidden, (((0,), (1,)), ((),...  43.8 us
    all_to_all x1, blocking collectives, local(): lax.all_to_all(outgoing, 'ep', split_axis=0, concat_axis=0, tiled=True)  32.7 us
    all_gather x1, waiting for transfers between devices, local(): lax.all_gather(head_mix, 'tp', axis=1, tiled=True)  23.4 us
    dot_general x1, matrix products, local(): lax.dot_general(down_local, hidden, (((0,), (1,)), ((), ())), preferred_e...  16.3 us
    dot_general x1, matrix products, local(): up_acc = jnp.dot(flat_piece, up_local, preferred_element_type=jnp.float32)  6.09 us
    all_to_all x1, starting transfers between devices, local(): lax.all_to_all(returned, 'ep', split_axis=1, concat_axis=1, tiled=True)  4.61 us
  transfers between devices with their start and end apart: 4, of which 2 were waited for; matrix products, arithmetic and copies ran while one was open for 4% of the time, Pallas kernels for 0%

profile of v1, /device:TPU:0, one launch (start us, length us, event | category | flops | bytes accessed | tf_op | source)
XLA Modules:
  0.0 224.5 jit_solution(3690234468721573864)
XLA Ops:
  7.2 0.0 copy-start
  7.2 0.0 copy-start.5
  7.2 0.0 reduce-scatter.2.cloned.1.call-start
  7.2 2.9 %convert_element_type.82 = f32[256,2048]{1,0:T(8,128)} convert(bf16[256,2048]{1,0:T(8,128)(2,1)} %param.17) | non-fusion elementwise | flops 524288 | bytes 3145728 | tf_op jit(solution)/shard_map/convert_element_type | solution.py:117
  10.1 1.5 multiply_reduce_fusion
  11.7 0.1 copy.83
  11.8 0.1 eq.39
  11.9 0.1 reshape.510
  12.1 1.1 reduce-window.6
  13.2 0.2 slice_reduce_fusion
  13.5 0.1 fusion.50
  13.6 0.3 select_reduce_fusion
  14.0 0.8 dynamic-slice
  14.7 1.1 fusion.25
  15.9 4.0 %gather_fusion = bf16[1024,512]{1,0:T(8,128)(2,1)S(1)} fusion(bf16[256,512]{1,0:T(8,128)(2,1)S(1)} %fusion.25, s32[1024]{0:T(1024)S(1)} %maximum_clamp_fusion), kind=kCustom, calls=%fused_computation | custom fusion | bytes 2101248 | tf_op jit(solution)/shard_map/jit(_take)/gather | solution.py:139
  19.8 0.5 select_select_fusion
  20.3 32.7 %all_to_all.15 = bf16[8,128,512]{2,1,0:T(8,128)(2,1)S(1)} all-to-all(bf16[8,128,512]{2,1,0:T(8,128)(2,1)S(1)} %select_select_fusion), channel_id=1, replica_groups=mesh['ep'=8,'tp'=4] {'ep'}, dimensions={0} | all-to-all | bytes 2097152 | tf_op jit(solution)/shard_map/all_to_all | solution.py:143
  53.0 0.7 copy.87
  53.8 0.5 stack.2
  54.3 0.0 copy-start.8
  54.3 51.3 %all_to_all.16 = bf16[4,8,128,512]{2,1,3,0:T(8,128)(2,1)S(1)} all-to-all(bf16[4,8,128,512]{2,1,3,0:T(8,128)(2,1)S(1)} %stack.2), channel_id=1, replica_groups=mesh['ep'=8,'tp'=4] {'tp'}, dimensions={0} | all-to-all | bytes 8388608 | tf_op jit(solution)/shard_map/all_to_all | solution.py:146
  105.6 2.0 copy-done.1
  107.6 6.1 %fusion = f32[1024,1024]{1,0:T(8,128)} fusion(bf16[1,2048,1024]{2,1,0:T(8,128)(2,1)S(1)} %copy-done.8, bf16[256,8,8,128]{3,2,1,0:T(8,128)(2,1)S(1)} %bitcast.130), kind=kOutput, calls=%fused_computation.2 | convolution fusion | flops 4294967296 | bytes 12582912 | tf_op jit(solution)/shard_map/dot_general | solution.py:150
  113.7 16.3 %convert_bitcast_fusion = bf16[2048,1024]{0,1:T(8,128)(2,1)} fusion(bf16[1,1024,2048]{2,1,0:T(8,128)(2,1)} %param.23, f32[1024,1024]{1,0:T(8,128)} %fusion, bf16[1,2048,1024]{2,1,0:T(8,128)(2,1)} %param.21, bf16[256,8,8,128]{3,2,1,0:T(8,128)(2,1)} %bitcast.131), kind=kOutput, calls=%fused_computation.10 | convolution fusion | flops 8598323200 | bytes 20971520 | tf_op jit(solution)/shard_map/dot_general | solution.py:153
  130.0 0.0 reduce-scatter.2.cloned.1.call-update
  130.0 0.0 copy-start.7
  130.0 0.0 all-gather.2.cloned.1.call-start
  130.1 0.8 copy-done.3
  130.8 0.1 copy-done.4
  130.9 0.1 constant_dynamic-slice_fusion
  131.1 0.1 copy.93
  131.2 0.1 copy.94
  131.3 0.3 fusion.44
  131.7 1.5 collective-permute-start
  133.2 0.1 copy.78
  133.4 0.1 broadcast_compare_fusion
  133.5 0.1 iota_add_fusion.1
  133.5 0.1 iota_add_fusion
  133.6 0.3 multiply_cosine_fusion
  133.9 0.3 fusion.27
  134.3 0.1 fusion.31
  134.5 0.0 collective-permute-done
  134.5 0.5 fusion.59
  135.0 0.1 broadcast_maximum_fusion
  135.1 0.3 fusion.21
  135.4 0.1 exponential_add_fusion
  135.5 0.5 fusion.22
  136.0 0.2 copy.82
  136.2 0.7 copy.122
  137.0 0.0 all-gather.2.cloned.1.call-update
  137.0 43.8 %reduce-scatter.2.cloned.1.call-done = bf16[512,1024]{0,1:T(8,128)(2,1)} async-done(((bf16[2048,1024]{0,1:T(8,128)(2,1)}), bf16[512,1024]{0,1:T(8,128)(2,1)}) %reduce-scatter.2.cloned.1.call-update) | async-done | bytes 1048592 | tf_op jit(solution)/shard_map/reduce_scatter | solution.py:152
  180.8 4.6 %all-to-all-start.2 = ((bf16[512,8,128]{0,2,1:T(8,128)(2,1)}), bf16[512,8,128]{0,2,1:T(8,128)(2,1)S(1)}, u32[]{:S(2)}, u32[]{:S(2)}) async-start(bf16[512,8,128]{0,2,1:T(8,128)(2,1)} %bitcast.134), calls=%async_computation.3 | async-start | bytes 2097152 | tf_op jit(solution)/shard_map/all_to_all | solution.py:161
  185.4 0.1 copy.88
  185.5 0.1 mul.228
  185.7 0.1 sub.79
  185.8 0.1 copy.85
  185.9 0.2 copy.86
  186.1 0.1 copy.89
  186.3 23.4 %all-gather.2.cloned.1.call-done = bf16[512,1024]{0,1:T(8,128)(2,1)} async-done(((bf16[512,256]{0,1:T(8,128)(2,1)}), bf16[512,1024]{0,1:T(8,128)(2,1)}) %all-gather.2.cloned.1.call-update) | async-done | bytes 1048592 | tf_op jit(solution)/shard_map/all_gather | solution.py:108
  209.7 2.7 %convolution_convert_fusion = bf16[512,512]{1,0:T(8,128)(2,1)} fusion(bf16[512,1024]{0,1:T(8,128)(2,1)} %all-gather.2.cloned.1.call-done, bf16[1024,512]{1,0:T(8,128)(2,1)S(1)} %copy-done), kind=kOutput, calls=%fused_computation.22 | convolution fusion | flops 537133056 | bytes 2621440 | tf_op jit(solution)/shard_map/dot_general | solution.py:107
  212.5 0.0 all-to-all-done.2
  212.5 2.0 gather_fusion.1
  214.5 0.2 gather.15
  214.7 2.9 %multiply_reduce_fusion.1 = bf16[512,256]{0,1:T(8,128)(2,1)} fusion(bf16[512,256,2]{0,2,1:T(2,128)(2,1)S(1)} %gather.15, pred[256,2]{1,0:T(8,128)(4,1)S(1)} %copy.86, f32[256,2]{1,0:T(8,128)S(1)} %copy.89), kind=kLoop, calls=%fused_computation.26 | loop fusion | flops 917504 | bytes 788992 | tf_op jit(solution)/shard_map/reduce_sum | solution.py:165
  (38 shorter events, 0.3 us)
Async XLA Ops:
  7.2 202.6 %copy-start = (bf16[1024,512]{1,0:T(8,128)(2,1)S(1)}, bf16[1024,512]{1,0:T(8,128)(2,1)}, u32[]{:S(2)}) copy-start(bf16[1024,512]{1,0:T(8,128)(2,1)} %param.16) | copy-start | bytes 3145732
  7.2 4.5 %copy-start.5 = (s32[256,2]{0,1:T(2,128)S(1)}, s32[256,2]{0,1:T(2,128)}, u32[]{:S(2)}) copy-start(s32[256,2]{0,1:T(2,128)} %param.19) | copy-start | bytes 6148
  7.2 173.6 %reduce-scatter.2.cloned.1.call-start = ((), (), s32[]{:S(2)}) async-start(), calls=%async_computation.5 | async-start | bytes 5242880 | tf_op jit(solution)/shard_map/reduce_scatter | solution.py:152
  54.3 53.2 %copy-start.8 = (bf16[1,2048,1024]{2,1,0:T(8,128)(2,1)S(1)}, bf16[1,2048,1024]{2,1,0:T(8,128)(2,1)}, u32[]{:S(2)}) copy-start(bf16[1,2048,1024]{2,1,0:T(8,128)(2,1)} %param.22) | copy-start | bytes 12582916
  105.6 2.0 copy-start.1
  129.9 0.9 copy-start.3
  129.9 1.0 copy-start.4
  129.9 3.2 %copy-start.2 = (bf16[512,256]{1,0:T(8,128)(2,1)S(1)}, bf16[512,256]{1,0:T(8,128)(2,1)}, u32[]{:S(2)}) copy-start(bf16[512,256]{1,0:T(8,128)(2,1)} %param.12) | copy-start | bytes 786436
  130.0 5.1 %copy-start.7 = (f32[4]{0:T(128)S(1)}, f32[4]{0:T(128)}, u32[]{:S(2)}) copy-start(f32[4]{0:T(128)} %param.15) | copy-start | bytes 52
  130.0 79.7 %all-gather.2.cloned.1.call-start = ((), (), s32[]{:S(2)}) async-start(), calls=%async_computation.4 | async-start | bytes 1310720 | tf_op jit(solution)/shard_map/all_gather | solution.py:108
  131.7 2.8 %collective-permute-start = (bf16[128,128]{0,1:T(8,128)(2,1)S(1)}, bf16[128,128]{0,1:T(8,128)(2,1)S(1)}, u32[]{:S(2)}, u32[]{:S(2)}) collective-permute-start(bf16[128,128]{0,1:T(8,128)(2,1)S(1)} %pad_maximum_fusion.3), channel_id=1, source_target_pairs={{0,4},{4,8},{8,12},{12,16},{16,20},{20,24},{24,28},{1,5},{5,9},{9,... | collective-permute-start | bytes 98312 | tf_op jit(solution)/shard_map/ppermute | solution.py:17
  135.5 50.6 %copy-start.6 = (f32[256,2]{0,1:T(2,128)S(1)}, f32[256,2]{0,1:T(2,128)}, u32[]{:S(2)}) copy-start(f32[256,2]{0,1:T(2,128)} %param.20) | copy-start | bytes 6148
  180.8 31.7 %all-to-all-start.2 = ((bf16[512,8,128]{0,2,1:T(8,128)(2,1)}), bf16[512,8,128]{0,2,1:T(8,128)(2,1)S(1)}, u32[]{:S(2)}, u32[]{:S(2)}) async-start(bf16[512,8,128]{0,2,1:T(8,128)(2,1)} %bitcast.134), calls=%async_computation.3 | async-start | bytes 2097152 | tf_op jit(solution)/shard_map/all_to_all | solution.py:161
Sparse Core Ops, SparseCore 0:
  130.1 50.6 reduce-scatter.1
  183.2 26.4 all-gather.1
